TPU v7x, 32 devices: a whole 2x2x4 slice. The times are simulated.
32 devices in a mesh: sp: 8 (over z, y), tp: 4 (over x, core).
Axes of the slice: x: 2, y: 2, z: 4, core: 2. Of those that a mesh axis runs over, the one named last changes fastest.
Arguments:
- residual_in: bfloat16 [8192, 2048], P(('sp', 'tp')), may hold values from -6 to 6
- queries: bfloat16 [8192, 2048], P('sp', 'tp'), may hold values from -200 to 200, as said below
- keys_values: bfloat16 [2, 8192, 1024], P(None, 'sp', 'tp'), may hold values from -6 to 6
- sink_logit: float32 [32], P('tp'), may hold values from -2 to 6
- out_weight: bfloat16 [2048, 2048], P('tp'), may hold values from -2 to 2
- norm1_gain: float32 [2048], replicated, may hold values from 0.1 to 1.9
- norm1_bias: float32 [2048], replicated, may hold values from -3 to 3
- up_weight: bfloat16 [2048, 8192], P('sp', 'tp'), may hold values from -0.125 to 0.125
- down_weight: bfloat16 [8192, 2048], P('tp', 'sp'), may hold values from -0.0625 to 0.0625
- norm2_gain: float32 [2048], replicated, may hold values from 0.1 to 1.9
- norm2_bias: float32 [2048], replicated, may hold values from -3 to 3
Outputs:
- stream_out: bfloat16 [8192, 2048], P(('sp', 'tp'))
Inputs may be any that keep to these rules, and one draw needn't show every extreme that they name: `queries`: of order one mostly; some rows may be large multiples of a nearby key row.
All inputs are finite; a program needn't handle non-finite values.
Results may differ from a plain program's by a relative error of at most 0.014.
Values may be sent and summed in bfloat16 or wider, within the bound.
A program may use at most 128 MiB of HBM per device.

v0:
```python
import jax
import jax.numpy as jnp
from jax import lax
from jax.sharding import PartitionSpec as P

HEAD_DIM = 64
WINDOW = 128


def with_halo(shard, sides, width):
    for axis, dim in sides:
        devices, length = (lax.axis_size(axis), shard.shape[dim])
        up = [(i, (i + 1) % devices) for i in range(devices - 1)]
        down = [(j, i) for i, j in up]
        last = lax.slice_in_dim(shard, length - width, length, axis=dim)
        first = lax.slice_in_dim(shard, 0, width, axis=dim)
        before = lax.ppermute(last, axis, up)
        after = lax.ppermute(first, axis, down)
        shard = jnp.concatenate([before, shard, after], axis=dim)
    return shard


def norm_rows(values, gain, bias):
    mean = jnp.mean(values, axis=-1, keepdims=True)
    centred = values - mean
    variance = jnp.mean(centred * centred, axis=-1, keepdims=True)
    return (centred * lax.rsqrt(variance + 1e-06) * gain + bias).astype(jnp.bfloat16)


def attend(queries, padded, sink_logit, offset, total):
    tok_rows = queries.shape[0]
    block = min(512, tok_rows)
    span = block + 2 * WINDOW
    kv_local = padded.shape[2] // HEAD_DIM
    heads_local = queries.shape[1] // HEAD_DIM
    group = heads_local // kv_local
    sink = sink_logit.reshape(kv_local, group, 1, 1)

    def one_block(index):
        start = index * block
        query = lax.dynamic_slice_in_dim(queries, start, block, 0).reshape(
            block, kv_local, group, HEAD_DIM
        )
        keys = lax.dynamic_slice_in_dim(padded[0], start, span, 0).reshape(span, kv_local, HEAD_DIM)
        values = lax.dynamic_slice_in_dim(padded[1], start, span, 0).reshape(
            span, kv_local, HEAD_DIM
        )
        scores = jnp.einsum(
            "qhgd,khd->hgqk", query, keys, preferred_element_type=jnp.float32
        ) * HEAD_DIM ** (-0.5)
        query_pos = offset + start + jnp.arange(block, dtype=jnp.int32)
        key_pos = offset + start - WINDOW + jnp.arange(span, dtype=jnp.int32)
        valid = (
            (jnp.abs(key_pos[None, :] - query_pos[:, None]) <= WINDOW)
            & (key_pos[None, :] >= 0)
            & (key_pos[None, :] < total)
        )
        scores = jnp.where(valid, scores, -jnp.inf)
        top = jnp.maximum(jnp.max(scores, axis=-1, keepdims=True), sink)
        expd = jnp.exp(scores - top)
        denom = jnp.sum(expd, axis=-1, keepdims=True) + jnp.exp(sink - top)
        weights = (expd / denom).astype(jnp.bfloat16)
        mixed = jnp.einsum("hgqk,khd->qhgd", weights, values, preferred_element_type=jnp.float32)
        return mixed.reshape(block, heads_local * HEAD_DIM).astype(jnp.bfloat16)

    blocks = lax.map(one_block, jnp.arange(tok_rows // block, dtype=jnp.int32))
    return blocks.reshape(tok_rows, heads_local * HEAD_DIM)


def activate(rows, up_full):
    hidden = jnp.dot(rows, up_full, preferred_element_type=jnp.float32)
    return jnp.square(jnp.maximum(hidden, 0.0)).astype(jnp.bfloat16)


def on_device(
    residual_in,
    queries,
    keys_values,
    sink_logit,
    out_weight,
    norm1_gain,
    norm1_bias,
    up_weight,
    down_weight,
    norm2_gain,
    norm2_bias,
):
    up_full, down_full = (
        lax.all_gather(up_weight, "sp", axis=0, tiled=True),
        lax.all_gather(down_weight, "sp", axis=1, tiled=True),
    )
    tok_rows = queries.shape[0]
    padded = with_halo(keys_values, (("sp", 1),), WINDOW)
    offset = lax.axis_index("sp") * tok_rows
    attended = attend(queries, padded, sink_logit, offset, tok_rows * lax.axis_size("sp"))
    rows = attended
    projected = lax.psum_scatter(
        jnp.dot(rows, out_weight, preferred_element_type=jnp.float32)
        .astype(jnp.bfloat16)
        .astype(jnp.float32)
        .astype(jnp.bfloat16),
        "tp",
        scatter_dimension=0,
        tiled=True,
    ).astype(jnp.float32)
    first = norm_rows(residual_in.astype(jnp.float32) + projected, norm1_gain, norm1_bias)
    activation = activate(lax.all_gather(first, "tp", axis=0, tiled=True), up_full)
    rows = activation
    branch = lax.psum_scatter(
        jnp.dot(rows, down_full, preferred_element_type=jnp.float32)
        .astype(jnp.bfloat16)
        .astype(jnp.float32)
        .astype(jnp.bfloat16),
        "tp",
        scatter_dimension=0,
        tiled=True,
    ).astype(jnp.float32)
    return norm_rows(first.astype(jnp.float32) + branch, norm2_gain, norm2_bias)


def solution(mesh):
    return jax.shard_map(
        on_device,
        mesh=mesh,
        in_specs=(
            P(("sp", "tp"), None),
            P("sp", "tp"),
            P(None, "sp", "tp"),
            P("tp"),
            P("tp", None),
            P(),
            P(),
            P("sp", "tp"),
            P("tp", "sp"),
            P(),
            P(),
        ),
        out_specs=P(("sp", "tp"), None),
        check_vma=False,
    )
```

profile of v0, /device:TPU:0, one launch (start us, length us, event | category | flops | bytes accessed | tf_op | source)
XLA Modules:
  0.0 449.1 jit_solution(10335722248176665415)
XLA Ops:
  7.4 1.6 copy.21
  9.7 4.9 %collective-permute-start = (bf16[2,128,256]{1,2,0:T(8,128)(2,1)}, bf16[2,128,256]{1,2,0:T(8,128)(2,1)S(1)}, u32[]{:S(2)}, u32[]{:S(2)}) collective-permute-start(bf16[2,128,256]{1,2,0:T(8,128)(2,1)} %get-tuple-element.131), channel_id=1, source_target_pairs={{0,4},{4,8},{8,12},{12,16},{16,20},{20,24},{24,28},{1,5},{5,9},{9,... | collective-permute-start | bytes 393224 | tf_op jit(solution)/shard_map/ppermute | solution.py:17
  14.6 1.3 collective-permute-start.1
  16.1 1.5 collective-permute-done
  17.7 3.8 collective-permute-done.1
  21.5 1.2 pad_maximum_fusion
  22.7 52.6 %while.12 = (s32[]{:T(128)}, bf16[2,512,512]{2,1,0:T(8,128)(2,1)}, bf16[2,1280,256]{1,2,0:T(8,128)(2,1)}, s32[2]{0:T(128)S(1)}, s32[]{:T(128)}, /*index=5*/bf16[...) while((s32[]{:T(128)}, bf16[2,512,512]{2,1,0:T(8,128)(2,1)}, ...), condition=%wide.region_3.4_spmd, body=%wide.region_0.3_spmd.sunk | while | flops 845295104 | bytes 101627824 | solution.py:66
  24.8 1.4 fusion.37
  26.2 1.0 constant_dynamic-slice_fusion.5
  27.2 1.1 constant_dynamic-slice_fusion.6
  28.5 7.6 %fusion.40 = (f32[4,2,512]{2,1,0:T(2,128)S(1)}, f32[4,768,512,2]{2,1,3,0:T(8,128)}) fusion(pred[512,768]{0,1:T(8,128)(4,1)S(1)} %fusion.39, bf16[768,4,64,1]{0,2,3,1:T(8,128)(2,1)} %bitcast.61, bf16[512,4,2,64]{0,3,2,1:T(8,128)(2,1)S(1)} %bitcast.60), kind=kOutput, calls=%fused_computation.4.clone.1 | convolution fusion | flops 412086272 | bytes 13910016 | tf_op jit(solution)/shard_map/while/body/eval_jaxpr/qhgd,khd->hgqk/dot_general | solution.py:48
  36.2 7.3 %fusion.41 = f32[4,2,512]{2,1,0:T(2,128)S(1)} fusion(f32[4,768,512,2]{2,1,3,0:T(8,128)} %get-tuple-element.190, f32[4,2,512]{2,1,0:T(2,128)S(1)} %broadcast_maximum_fusion.2, pred[512,768]{0,1:T(8,128)(4,1)S(1)} %fusion.39), kind=kLoop, calls=%fused_computation.3.clone.1 | loop fusion | flops 12578816 | bytes 13008896 | tf_op jit(solution)/shard_map/while/body/eval_jaxpr/reduce_sum | solution.py:61
  44.4 3.6 fusion.42
  48.2 0.8 constant_dynamic-update-slice_fusion.2
  51.1 1.4 fusion.37
  52.5 1.0 constant_dynamic-slice_fusion.5
  53.5 1.1 constant_dynamic-slice_fusion.6
  54.8 7.6 %fusion.40 = (f32[4,2,512]{2,1,0:T(2,128)S(1)}, f32[4,768,512,2]{2,1,3,0:T(8,128)}) fusion(pred[512,768]{0,1:T(8,128)(4,1)S(1)} %fusion.39, bf16[768,4,64,1]{0,2,3,1:T(8,128)(2,1)} %bitcast.61, bf16[512,4,2,64]{0,3,2,1:T(8,128)(2,1)S(1)} %bitcast.60), kind=kOutput, calls=%fused_computation.4.clone.1 | convolution fusion | flops 412086272 | bytes 13910016 | tf_op jit(solution)/shard_map/while/body/eval_jaxpr/qhgd,khd->hgqk/dot_general | solution.py:48
  62.5 7.3 %fusion.41 = f32[4,2,512]{2,1,0:T(2,128)S(1)} fusion(f32[4,768,512,2]{2,1,3,0:T(8,128)} %get-tuple-element.190, f32[4,2,512]{2,1,0:T(2,128)S(1)} %broadcast_maximum_fusion.2, pred[512,768]{0,1:T(8,128)(4,1)S(1)} %fusion.39), kind=kLoop, calls=%fused_computation.3.clone.1 | loop fusion | flops 12578816 | bytes 13008896 | tf_op jit(solution)/shard_map/while/body/eval_jaxpr/reduce_sum | solution.py:61
  70.7 3.6 fusion.42
  74.5 0.8 constant_dynamic-update-slice_fusion.2
  75.3 5.5 %convolution_convert_fusion.1 = bf16[1024,2048]{1,0:T(8,128)(2,1)} fusion(bf16[1024,512]{1,0:T(8,128)(2,1)} %bitcast.65, bf16[512,2048]{1,0:T(8,128)(2,1)S(1)} %copy-done), kind=kOutput, calls=%fused_computation.24 | convolution fusion | flops 2149580800 | bytes 7340032 | tf_op jit(solution)/shard_map/dot_general | solution.py:98
  82.1 44.6 %reduce-scatter.3.cloned.1.call-done = bf16[256,2048]{1,0:T(8,128)(2,1)} async-done(((bf16[1024,2048]{1,0:T(8,128)(2,1)}), bf16[256,2048]{1,0:T(8,128)(2,1)}) %reduce-scatter.3.cloned.1.call-update) | async-done | bytes 1048592 | tf_op jit(solution)/shard_map/reduce_scatter | solution.py:97
  126.7 1.7 fusion.11
  129.0 1.5 add_convert_fusion.1
  130.8 78.1 %all-gather.6.cloned.1.call-done = bf16[2048,2048]{1,0:T(8,128)(2,1)} async-done(((bf16[256,2048]{1,0:T(8,128)(2,1)}), bf16[2048,2048]{1,0:T(8,128)(2,1)}) %all-gather.6.cloned.1.call-update) | async-done | bytes 8388624 | tf_op jit(solution)/shard_map/all_gather | solution.py:89
  208.8 124.8 %all-gather.8.cloned.1.call-done = bf16[2048,2048]{1,0:T(8,128)(2,1)} async-done(((bf16[2048,256]{1,0:T(8,128)(2,1)}), bf16[2048,2048]{1,0:T(8,128)(2,1)}) %all-gather.8.cloned.1.call-update) | async-done | bytes 8388624 | tf_op jit(solution)/shard_map/all_gather | solution.py:90
  333.7 34.0 %all-gather.4.cloned.1.call-done = bf16[1024,2048]{1,0:T(8,128)(2,1)} async-done(((bf16[256,2048]{1,0:T(8,128)(2,1)}), bf16[1024,2048]{1,0:T(8,128)(2,1)}) %all-gather.4.cloned.1.call-update) | async-done | bytes 4194320 | tf_op jit(solution)/shard_map/all_gather | solution.py:107
  367.6 25.4 %convolution_convert_fusion = bf16[1024,2048]{1,0:T(8,128)(2,1)} fusion(bf16[2048,2048]{1,0:T(8,128)(2,1)} %all-gather.8.cloned.1.call-done, bf16[1024,2048]{1,0:T(8,128)(2,1)} %all-gather.4.cloned.1.call-done, bf16[2048,2048]{1,0:T(8,128)(2,1)} %all-gather.6.cloned.1.call-done), kind=kOutput, calls=%fused_computation.23 | convolution fusion | flops 17188257792 | bytes 25165824 | tf_op jit(solution)/shard_map/dot_general | solution.py:110
  393.0 44.7 %reduce-scatter.5.cloned.1.call-done = bf16[256,2048]{1,0:T(8,128)(2,1)} async-done(((bf16[1024,2048]{1,0:T(8,128)(2,1)}), bf16[256,2048]{1,0:T(8,128)(2,1)}) %reduce-scatter.5.cloned.1.call-update) | async-done | bytes 1048592 | tf_op jit(solution)/shard_map/reduce_scatter | solution.py:109
  437.8 1.7 fusion.13
  440.0 1.5 add_convert_fusion
  (69 shorter events, 9.1 us)
Async XLA Ops:
  7.4 68.0 %copy-start = (bf16[512,2048]{1,0:T(8,128)(2,1)S(1)}, bf16[512,2048]{1,0:T(8,128)(2,1)}, u32[]{:S(2)}) copy-start(bf16[512,2048]{1,0:T(8,128)(2,1)} %param.17) | copy-start | bytes 6291460
  7.4 8.6 %copy-start.11 = (f32[8]{0:T(128)S(1)}, f32[8]{0:T(128)}, u32[]{:S(2)}) copy-start(f32[8]{0:T(128)} %param.16) | copy-start | bytes 100
  7.4 119.3 %reduce-scatter.3.cloned.1.call-start = ((), (), s32[]{:S(2)}) async-start(), calls=%async_computation.2 | async-start | bytes 5242880 | tf_op jit(solution)/shard_map/reduce_scatter | solution.py:97
  9.7 7.9 %collective-permute-start = (bf16[2,128,256]{1,2,0:T(8,128)(2,1)}, bf16[2,128,256]{1,2,0:T(8,128)(2,1)S(1)}, u32[]{:S(2)}, u32[]{:S(2)}) collective-permute-start(bf16[2,128,256]{1,2,0:T(8,128)(2,1)} %get-tuple-element.131), channel_id=1, source_target_pairs={{0,4},{4,8},{8,12},{12,16},{16,20},{20,24},{24,28},{1,5},{5,9},{9,... | collective-permute-start | bytes 393224 | tf_op jit(solution)/shard_map/ppermute | solution.py:17
  14.6 6.9 %collective-permute-start.1 = (bf16[2,128,256]{1,2,0:T(8,128)(2,1)S(1)}, bf16[2,128,256]{1,2,0:T(8,128)(2,1)S(1)}, u32[]{:S(2)}, u32[]{:S(2)}) collective-permute-start(bf16[2,128,256]{1,2,0:T(8,128)(2,1)S(1)} %get-tuple-element.132), channel_id=1, source_target_pairs={{4,0},{8,4},{12,8},{16,12},{20,16},{24,20},{28,24},{5,1},{9,5},{13... | collective-permute-start | bytes 393224 | tf_op jit(solution)/shard_map/ppermute | solution.py:18
  36.2 8.2 %copy-start.1 = (f32[4,768,512,2]{2,1,3,0:T(8,128)S(1)}, f32[4,768,512,2]{2,1,3,0:T(8,128)}, u32[]{:S(2)}) copy-start(f32[4,768,512,2]{2,1,3,0:T(8,128)} %get-tuple-element.190) | copy-start | bytes 37748740 | tf_op jit(solution)/shard_map/while
  36.2 8.2 %copy-start.3 = (bf16[1,768,256]{1,2,0:T(8,128)(2,1)S(1)}, bf16[1,768,256]{1,2,0:T(8,128)(2,1)}, u32[]{:S(2)}) copy-start(bf16[1,768,256]{1,2,0:T(8,128)(2,1)} %get-tuple-element.186) | copy-start | bytes 1179652 | tf_op jit(solution)/shard_map/while
  62.5 8.2 %copy-start.1 = (f32[4,768,512,2]{2,1,3,0:T(8,128)S(1)}, f32[4,768,512,2]{2,1,3,0:T(8,128)}, u32[]{:S(2)}) copy-start(f32[4,768,512,2]{2,1,3,0:T(8,128)} %get-tuple-element.190) | copy-start | bytes 37748740 | tf_op jit(solution)/shard_map/while
  62.5 8.2 %copy-start.3 = (bf16[1,768,256]{1,2,0:T(8,128)(2,1)S(1)}, bf16[1,768,256]{1,2,0:T(8,128)(2,1)}, u32[]{:S(2)}) copy-start(bf16[1,768,256]{1,2,0:T(8,128)(2,1)} %get-tuple-element.186) | copy-start | bytes 1179652 | tf_op jit(solution)/shard_map/while
  80.8 45.9 %copy-start.4 = (bf16[256,2048]{1,0:T(8,128)(2,1)S(1)}, bf16[256,2048]{1,0:T(8,128)(2,1)}, u32[]{:S(2)}) copy-start(bf16[256,2048]{1,0:T(8,128)(2,1)} %param.13) | copy-start | bytes 3145732
  80.9 127.9 %all-gather.6.cloned.1.call-start = ((), (), s32[]{:S(2)}) async-start(), calls=%async_computation.4 | async-start | bytes 9437184 | tf_op jit(solution)/shard_map/all_gather | solution.py:89
  81.5 47.5 %copy-start.7 = (f32[2048]{0:T(1024)S(1)}, f32[2048]{0:T(1024)}, u32[]{:S(2)}) copy-start(f32[2048]{0:T(1024)} %param.19) | copy-start | bytes 24580
  81.5 47.5 %copy-start.8 = (f32[2048]{0:T(1024)S(1)}, f32[2048]{0:T(1024)}, u32[]{:S(2)}) copy-start(f32[2048]{0:T(1024)} %param.18) | copy-start | bytes 24580
  81.5 252.2 %all-gather.8.cloned.1.call-start = ((), (), s32[]{:S(2)}) async-start(), calls=%async_computation.5 | async-start | bytes 9437184 | tf_op jit(solution)/shard_map/all_gather | solution.py:90
  82.1 285.5 %all-gather.4.cloned.1.call-start = ((), (), s32[]{:S(2)}) async-start(), calls=%async_computation.3 | async-start | bytes 5242880 | tf_op jit(solution)/shard_map/all_gather | solution.py:107
  126.7 1.7 copy-start.5
  130.5 307.3 %reduce-scatter.5.cloned.1.call-start = ((), (), s32[]{:S(2)}) async-start(), calls=%async_computation.6 | async-start | bytes 5242880 | tf_op jit(solution)/shard_map/reduce_scatter | solution.py:109
  393.0 44.8 %copy-start.2 = (bf16[256,2048]{1,0:T(8,128)(2,1)S(1)}, bf16[256,2048]{1,0:T(8,128)(2,1)}, u32[]{:S(2)}) copy-start(bf16[256,2048]{1,0:T(8,128)(2,1)} %add_convert_fusion.1) | copy-start | bytes 3145732
  393.0 47.0 %copy-start.9 = (f32[2048]{0:T(1024)S(1)}, f32[2048]{0:T(1024)}, u32[]{:S(2)}) copy-start(f32[2048]{0:T(1024)} %param.23) | copy-start | bytes 24580
  393.0 47.0 %copy-start.10 = (f32[2048]{0:T(1024)S(1)}, f32[2048]{0:T(1024)}, u32[]{:S(2)}) copy-start(f32[2048]{0:T(1024)} %param.22) | copy-start | bytes 24580
  437.8 1.7 copy-start.6
Sparse Core Ops, SparseCore 0:
  81.0 45.6 reduce-scatter.2
  393.1 44.5 reduce-scatter.4
Sparse Core Ops, SparseCore 1:
  83.5 125.3 all-gather.5
  210.7 122.9 all-gather.7
  335.1 32.5 all-gather.3
where the time goes:
time: 450 us; the launch traced here: 449 us
  waiting for transfers between devices  333 us (74%)
  matrix products  53.3 us (12%)
  other arithmetic  25.3 us (6%)
  between operations  15.2 us (3%)
  local copies, waits for them, and re-layouts  14.8 us (3%)
  starting transfers between devices  6.54 us (1%)
    all_gather x1, waiting for transfers between devices, on_device(): lax.all_gather(down_weight, 'sp', axis=1, tiled=True)  125 us
    all_gather x1, waiting for transfers between devices, on_device(): lax.all_gather(up_weight, 'sp', axis=0, tiled=True)  78.1 us
    reduce_scatter x1, waiting for transfers between devices, on_device(): lax.psum_scatter(jnp.dot(rows, down_full, preferred_element_type=jnp.floa...  44.7 us
    reduce_scatter x1, waiting for transfers between devices, on_device(): lax.psum_scatter(jnp.dot(rows, out_weight, preferred_element_type=jnp.flo...  44.6 us
    all_gather x1, waiting for transfers between devices, on_device(): lax.all_gather(first, 'tp', axis=0, tiled=True)  34 us
    dot_general x1, matrix products, on_device(): jnp.dot(rows, down_full, preferred_element_type=jnp.float32)  25.4 us
    dot_general x2, matrix products, one_block(): jnp.einsum('qhgd,khd->hgqk', query, keys, preferred_element_type=jnp.floa...  15.2 us
    reduce_sum x2, other arithmetic, one_block(): denom = jnp.sum(expd, axis=-1, keepdims=True) + jnp.exp(sink - top)  14.7 us
  transfers between devices with their start and end apart: 7, of which 7 were waited for; matrix products, arithmetic and copies ran while one was open for 1% of the time, Pallas kernels for 0%

commit v1 on v0

--- a/solution.py
+++ b/solution.py
@@ -1,3 +1,4 @@
+import functools
 import jax
 import jax.numpy as jnp
 from jax import lax
@@ -5,6 +6,13 @@
 
 HEAD_DIM = 64
 WINDOW = 128
+
+
+def ends_derive(sample, dimension_no):
+    return jnp.concatenate(lax.all_gather(sample, axis_name="sp"), axis=dimension_no)
+
+
+_assign_groups = functools.partial(ends_derive, dimension_no=1)
 
 
 def with_halo(shard, sides, width):
@@ -87,7 +95,7 @@
 ):
     up_full, down_full = (
         lax.all_gather(up_weight, "sp", axis=0, tiled=True),
-        lax.all_gather(down_weight, "sp", axis=1, tiled=True),
+        _assign_groups(down_weight),
     )
     tok_rows = queries.shape[0]
     padded = with_halo(keys_values, (("sp", 1),), WINDOW)

time: 450 us -> 449 us (level)
  waiting for transfers between devices: 333 us -> 320 us
  local copies, waits for them, and re-layouts: 14.8 us -> 26.6 us
    all_gather x1, waiting for transfers between devices: 125 us -> 78.1 us  [ends_derive(): lax.all_gather(sample, axis_name='sp')]
    all_gather x1, waiting for transfers between devices: 78.1 us -> 113 us  [on_device(): lax.all_gather(up_weight, 'sp', axis=0, tiled=True)]
    reshape x0 -> x1, local copies, waits for them, and re-layouts: none -> 11.7 us  [ends_derive(): jnp.concatenate(lax.all_gather(sample, axis_name='sp'), axis=dimension_no)]
  transfers between devices with their start and end apart: 7 -> 7, of which waited for: 7 -> 7; matrix products, arithmetic and copies ran while one was open for 1% -> 3% of each run, Pallas kernels for 0% -> 0%
where the time goes in v1:
time: 449 us
  waiting for transfers between devices  320 us (71%)
  matrix products  53.3 us (12%)
  local copies, waits for them, and re-layouts  26.6 us (6%)
  other arithmetic  25.3 us (6%)
  between operations  15.2 us (3%)
  starting transfers between devices  6.54 us (1%)
    all_gather x1, waiting for transfers between devices, on_device(): lax.all_gather(up_weight, 'sp', axis=0, tiled=True)  113 us
    all_gather x1, waiting for transfers between devices, ends_derive(): lax.all_gather(sample, axis_name='sp')  78.1 us
    reduce_scatter x1, waiting for transfers between devices, on_device(): lax.psum_scatter(jnp.dot(rows, down_full, preferred_element_type=jnp.floa...  44.7 us
    reduce_scatter x1, waiting for transfers between devices, on_device(): lax.psum_scatter(jnp.dot(rows, out_weight, preferred_element_type=jnp.flo...  44.6 us
    all_gather x1, waiting for transfers between devices, on_device(): lax.all_gather(first, 'tp', axis=0, tiled=True)  34 us
    dot_general x1, matrix products, on_device(): jnp.dot(rows, down_full, preferred_element_type=jnp.float32)  25.4 us
    dot_general x2, matrix products, one_block(): jnp.einsum('qhgd,khd->hgqk', query, keys, preferred_element_type=jnp.floa...  15.2 us
    reduce_sum x2, other arithmetic, one_block(): denom = jnp.sum(expd, axis=-1, keepdims=True) + jnp.exp(sink - top)  14.7 us
  transfers between devices with their start and end apart: 7, of which 7 were waited for; matrix products, arithmetic and copies ran while one was open for 3% of the time, Pallas kernels for 0%

profile of v1, /device:TPU:0, one launch (start us, length us, event | category | flops | bytes accessed | tf_op | source)
XLA Modules:
  0.0 448.6 jit_solution(3657825355428759963)
XLA Ops:
  7.4 1.6 copy.29
  9.7 4.9 %collective-permute-start = (bf16[2,128,256]{1,2,0:T(8,128)(2,1)}, bf16[2,128,256]{1,2,0:T(8,128)(2,1)S(1)}, u32[]{:S(2)}, u32[]{:S(2)}) collective-permute-start(bf16[2,128,256]{1,2,0:T(8,128)(2,1)} %get-tuple-element.138), channel_id=1, source_target_pairs={{0,4},{4,8},{8,12},{12,16},{16,20},{20,24},{24,28},{1,5},{5,9},{9,... | collective-permute-start | bytes 393224 | tf_op jit(solution)/shard_map/ppermute | solution.py:25
  14.6 1.3 collective-permute-start.1
  16.1 1.5 collective-permute-done
  17.7 3.8 collective-permute-done.1
  21.5 1.2 pad_maximum_fusion
  22.7 52.6 %while.12 = (s32[]{:T(128)}, bf16[2,512,512]{2,1,0:T(8,128)(2,1)}, bf16[2,1280,256]{1,2,0:T(8,128)(2,1)}, s32[2]{0:T(128)S(1)}, s32[]{:T(128)}, /*index=5*/bf16[...) while((s32[]{:T(128)}, bf16[2,512,512]{2,1,0:T(8,128)(2,1)}, ...), condition=%wide.region_3.4_spmd, body=%wide.region_0.3_spmd.sunk | while | flops 845295104 | bytes 101627824 | solution.py:74
  24.8 1.4 fusion.37
  26.2 1.0 constant_dynamic-slice_fusion.5
  27.2 1.1 constant_dynamic-slice_fusion.6
  28.5 7.6 %fusion.40 = (f32[4,2,512]{2,1,0:T(2,128)S(1)}, f32[4,768,512,2]{2,1,3,0:T(8,128)}) fusion(pred[512,768]{0,1:T(8,128)(4,1)S(1)} %fusion.39, bf16[768,4,64,1]{0,2,3,1:T(8,128)(2,1)} %bitcast.65, bf16[512,4,2,64]{0,3,2,1:T(8,128)(2,1)S(1)} %bitcast.64), kind=kOutput, calls=%fused_computation.4.clone.1 | convolution fusion | flops 412086272 | bytes 13910016 | tf_op jit(solution)/shard_map/while/body/eval_jaxpr/qhgd,khd->hgqk/dot_general | solution.py:56
  36.2 7.3 %fusion.41 = f32[4,2,512]{2,1,0:T(2,128)S(1)} fusion(f32[4,768,512,2]{2,1,3,0:T(8,128)} %get-tuple-element.197, f32[4,2,512]{2,1,0:T(2,128)S(1)} %broadcast_maximum_fusion.2, pred[512,768]{0,1:T(8,128)(4,1)S(1)} %fusion.39), kind=kLoop, calls=%fused_computation.3.clone.1 | loop fusion | flops 12578816 | bytes 13008896 | tf_op jit(solution)/shard_map/while/body/eval_jaxpr/reduce_sum | solution.py:69
  44.4 3.6 fusion.42
  48.2 0.8 constant_dynamic-update-slice_fusion.2
  51.1 1.4 fusion.37
  52.5 1.0 constant_dynamic-slice_fusion.5
  53.5 1.1 constant_dynamic-slice_fusion.6
  54.8 7.6 %fusion.40 = (f32[4,2,512]{2,1,0:T(2,128)S(1)}, f32[4,768,512,2]{2,1,3,0:T(8,128)}) fusion(pred[512,768]{0,1:T(8,128)(4,1)S(1)} %fusion.39, bf16[768,4,64,1]{0,2,3,1:T(8,128)(2,1)} %bitcast.65, bf16[512,4,2,64]{0,3,2,1:T(8,128)(2,1)S(1)} %bitcast.64), kind=kOutput, calls=%fused_computation.4.clone.1 | convolution fusion | flops 412086272 | bytes 13910016 | tf_op jit(solution)/shard_map/while/body/eval_jaxpr/qhgd,khd->hgqk/dot_general | solution.py:56
  62.5 7.3 %fusion.41 = f32[4,2,512]{2,1,0:T(2,128)S(1)} fusion(f32[4,768,512,2]{2,1,3,0:T(8,128)} %get-tuple-element.197, f32[4,2,512]{2,1,0:T(2,128)S(1)} %broadcast_maximum_fusion.2, pred[512,768]{0,1:T(8,128)(4,1)S(1)} %fusion.39), kind=kLoop, calls=%fused_computation.3.clone.1 | loop fusion | flops 12578816 | bytes 13008896 | tf_op jit(solution)/shard_map/while/body/eval_jaxpr/reduce_sum | solution.py:69
  70.7 3.6 fusion.42
  75.3 5.5 %convolution_convert_fusion.1 = bf16[1024,2048]{1,0:T(8,128)(2,1)} fusion(bf16[1024,512]{1,0:T(8,128)(2,1)} %bitcast.71, bf16[512,2048]{1,0:T(8,128)(2,1)S(1)} %copy-done), kind=kOutput, calls=%fused_computation.24 | convolution fusion | flops 2149580800 | bytes 7340032 | tf_op jit(solution)/shard_map/dot_general | solution.py:106
  82.1 44.6 %reduce-scatter.3.cloned.1.call-done = bf16[256,2048]{1,0:T(8,128)(2,1)} async-done(((bf16[1024,2048]{1,0:T(8,128)(2,1)}), bf16[256,2048]{1,0:T(8,128)(2,1)}) %reduce-scatter.3.cloned.1.call-update) | async-done | bytes 1048592 | tf_op jit(solution)/shard_map/reduce_scatter | solution.py:105
  126.7 1.7 fusion.11
  129.0 1.5 add_convert_fusion.1
  130.8 78.1 %all-gather.9.cloned.1.call-done = bf16[16384,256]{1,0:T(8,128)(2,1)} async-done(((bf16[2048,256]{1,0:T(8,128)(2,1)}), bf16[16384,256]{1,0:T(8,128)(2,1)}) %all-gather.9.cloned.1.call-update) | async-done | bytes 8388624 | tf_op jit(solution)/shard_map/all_gather | solution.py:12
  208.8 11.7 %copy.35 = bf16[2048,8,256]{0,2,1:T(8,128)(2,1)} copy(bf16[2048,8,256]{2,0,1:T(8,128)(2,1)} %bitcast.68) | data formatting | bytes 16777216 | tf_op jit(solution)/shard_map/reshape | solution.py:12
  220.6 112.6 %all-gather.7.cloned.1.call-done = bf16[2048,2048]{1,0:T(8,128)(2,1)} async-done(((bf16[256,2048]{1,0:T(8,128)(2,1)}), bf16[2048,2048]{1,0:T(8,128)(2,1)}) %all-gather.7.cloned.1.call-update) | async-done | bytes 8388624 | tf_op jit(solution)/shard_map/all_gather | solution.py:97
  333.2 34.0 %all-gather.5.cloned.1.call-done = bf16[1024,2048]{1,0:T(8,128)(2,1)} async-done(((bf16[256,2048]{1,0:T(8,128)(2,1)}), bf16[1024,2048]{1,0:T(8,128)(2,1)}) %all-gather.5.cloned.1.call-update) | async-done | bytes 4194320 | tf_op jit(solution)/shard_map/all_gather | solution.py:115
  367.1 25.4 %convolution_convert_fusion = bf16[1024,2048]{1,0:T(8,128)(2,1)} fusion(bf16[2048,2048]{0,1:T(8,128)(2,1)} %bitcast.69, bf16[1024,2048]{1,0:T(8,128)(2,1)} %all-gather.5.cloned.1.call-done, bf16[2048,2048]{1,0:T(8,128)(2,1)} %all-gather.7.cloned.1.call-done), kind=kOutput, calls=%fused_computation.23 | convolution fusion | flops 17188257792 | bytes 25165824 | tf_op jit(solution)/shard_map/dot_general | solution.py:118
  392.6 44.7 %reduce-scatter.5.cloned.1.call-done = bf16[256,2048]{1,0:T(8,128)(2,1)} async-done(((bf16[1024,2048]{1,0:T(8,128)(2,1)}), bf16[256,2048]{1,0:T(8,128)(2,1)}) %reduce-scatter.5.cloned.1.call-update) | async-done | bytes 1048592 | tf_op jit(solution)/shard_map/reduce_scatter | solution.py:117
  437.3 1.7 fusion.13
  439.5 1.5 add_convert_fusion
  (70 shorter events, 10.0 us)
Async XLA Ops:
  7.4 68.0 %copy-start = (bf16[512,2048]{1,0:T(8,128)(2,1)S(1)}, bf16[512,2048]{1,0:T(8,128)(2,1)}, u32[]{:S(2)}) copy-start(bf16[512,2048]{1,0:T(8,128)(2,1)} %param.17) | copy-start | bytes 6291460
  7.4 8.6 %copy-start.11 = (f32[8]{0:T(128)S(1)}, f32[8]{0:T(128)}, u32[]{:S(2)}) copy-start(f32[8]{0:T(128)} %param.16) | copy-start | bytes 100
  7.4 119.3 %reduce-scatter.3.cloned.1.call-start = ((), (), s32[]{:S(2)}) async-start(), calls=%async_computation.2 | async-start | bytes 5242880 | tf_op jit(solution)/shard_map/reduce_scatter | solution.py:105
  9.7 7.9 %collective-permute-start = (bf16[2,128,256]{1,2,0:T(8,128)(2,1)}, bf16[2,128,256]{1,2,0:T(8,128)(2,1)S(1)}, u32[]{:S(2)}, u32[]{:S(2)}) collective-permute-start(bf16[2,128,256]{1,2,0:T(8,128)(2,1)} %get-tuple-element.138), channel_id=1, source_target_pairs={{0,4},{4,8},{8,12},{12,16},{16,20},{20,24},{24,28},{1,5},{5,9},{9,... | collective-permute-start | bytes 393224 | tf_op jit(solution)/shard_map/ppermute | solution.py:25
  14.6 6.9 %collective-permute-start.1 = (bf16[2,128,256]{1,2,0:T(8,128)(2,1)S(1)}, bf16[2,128,256]{1,2,0:T(8,128)(2,1)S(1)}, u32[]{:S(2)}, u32[]{:S(2)}) collective-permute-start(bf16[2,128,256]{1,2,0:T(8,128)(2,1)S(1)} %get-tuple-element.139), channel_id=1, source_target_pairs={{4,0},{8,4},{12,8},{16,12},{20,16},{24,20},{28,24},{5,1},{9,5},{13... | collective-permute-start | bytes 393224 | tf_op jit(solution)/shard_map/ppermute | solution.py:26
  36.2 8.2 %copy-start.1 = (f32[4,768,512,2]{2,1,3,0:T(8,128)S(1)}, f32[4,768,512,2]{2,1,3,0:T(8,128)}, u32[]{:S(2)}) copy-start(f32[4,768,512,2]{2,1,3,0:T(8,128)} %get-tuple-element.197) | copy-start | bytes 37748740 | tf_op jit(solution)/shard_map/while
  36.2 8.2 %copy-start.3 = (bf16[1,768,256]{1,2,0:T(8,128)(2,1)S(1)}, bf16[1,768,256]{1,2,0:T(8,128)(2,1)}, u32[]{:S(2)}) copy-start(bf16[1,768,256]{1,2,0:T(8,128)(2,1)} %get-tuple-element.193) | copy-start | bytes 1179652 | tf_op jit(solution)/shard_map/while
  62.5 8.2 %copy-start.1 = (f32[4,768,512,2]{2,1,3,0:T(8,128)S(1)}, f32[4,768,512,2]{2,1,3,0:T(8,128)}, u32[]{:S(2)}) copy-start(f32[4,768,512,2]{2,1,3,0:T(8,128)} %get-tuple-element.197) | copy-start | bytes 37748740 | tf_op jit(solution)/shard_map/while
  62.5 8.2 %copy-start.3 = (bf16[1,768,256]{1,2,0:T(8,128)(2,1)S(1)}, bf16[1,768,256]{1,2,0:T(8,128)(2,1)}, u32[]{:S(2)}) copy-start(bf16[1,768,256]{1,2,0:T(8,128)(2,1)} %get-tuple-element.193) | copy-start | bytes 1179652 | tf_op jit(solution)/shard_map/while
  80.8 45.9 %copy-start.4 = (bf16[256,2048]{1,0:T(8,128)(2,1)S(1)}, bf16[256,2048]{1,0:T(8,128)(2,1)}, u32[]{:S(2)}) copy-start(bf16[256,2048]{1,0:T(8,128)(2,1)} %param.13) | copy-start | bytes 3145732
  80.9 127.9 %all-gather.9.cloned.1.call-start = ((), (), s32[]{:S(2)}) async-start(), calls=%async_computation.6 | async-start | bytes 9437184 | tf_op jit(solution)/shard_map/all_gather | solution.py:12
  81.5 47.5 %copy-start.7 = (f32[2048]{0:T(1024)S(1)}, f32[2048]{0:T(1024)}, u32[]{:S(2)}) copy-start(f32[2048]{0:T(1024)} %param.19) | copy-start | bytes 24580
  81.5 47.5 %copy-start.8 = (f32[2048]{0:T(1024)S(1)}, f32[2048]{0:T(1024)}, u32[]{:S(2)}) copy-start(f32[2048]{0:T(1024)} %param.18) | copy-start | bytes 24580
  81.5 251.7 %all-gather.7.cloned.1.call-start = ((), (), s32[]{:S(2)}) async-start(), calls=%async_computation.4 | async-start | bytes 9437184 | tf_op jit(solution)/shard_map/all_gather | solution.py:97
  82.1 285.1 %all-gather.5.cloned.1.call-start = ((), (), s32[]{:S(2)}) async-start(), calls=%async_computation.3 | async-start | bytes 5242880 | tf_op jit(solution)/shard_map/all_gather | solution.py:115
  126.7 1.7 copy-start.5
  130.5 306.8 %reduce-scatter.5.cloned.1.call-start = ((), (), s32[]{:S(2)}) async-start(), calls=%async_computation.5 | async-start | bytes 5242880 | tf_op jit(solution)/shard_map/reduce_scatter | solution.py:117
  392.5 44.8 %copy-start.2 = (bf16[256,2048]{1,0:T(8,128)(2,1)S(1)}, bf16[256,2048]{1,0:T(8,128)(2,1)}, u32[]{:S(2)}) copy-start(bf16[256,2048]{1,0:T(8,128)(2,1)} %add_convert_fusion.1) | copy-start | bytes 3145732
  392.5 47.0 %copy-start.9 = (f32[2048]{0:T(1024)S(1)}, f32[2048]{0:T(1024)}, u32[]{:S(2)}) copy-start(f32[2048]{0:T(1024)} %param.23) | copy-start | bytes 24580
  392.5 47.0 %copy-start.10 = (f32[2048]{0:T(1024)S(1)}, f32[2048]{0:T(1024)}, u32[]{:S(2)}) copy-start(f32[2048]{0:T(1024)} %param.22) | copy-start | bytes 24580
  437.3 1.7 copy-start.6
Sparse Core Ops, SparseCore 0:
  81.0 45.6 reduce-scatter.2
  392.7 44.5 reduce-scatter.4
Sparse Core Ops, SparseCore 1:
  83.5 125.3 all-gather.8
  210.8 122.3 all-gather.6
  334.6 32.5 all-gather.4
